TPU v7x, 32 devices: a whole 2x2x4 slice. The times are simulated.
32 devices in a mesh: kv: 8 (over z, y), tp: 4 (over x, core).
Axes of the slice: x: 2, y: 2, z: 4, core: 2. Of those that a mesh axis runs over, the one named last changes fastest.
Arguments:
- tokens: bfloat16 [16, 4096], P(None, ('kv', 'tp')), may hold values from -6 to 6
- gain_attn: bfloat16 [4096], replicated, may hold values from 0.099609375 to 1.8984375
- w_query: bfloat16 [4096, 2048], P('kv', 'tp'), may hold values from -0.09375 to 0.09375
- w_key: bfloat16 [4096, 2048], P('kv', 'tp'), may hold values from -0.09375 to 0.09375
- w_value: bfloat16 [4096, 2048], P('kv', 'tp'), may hold values from -0.09375 to 0.09375
- w_forget: bfloat16 [4096, 32], replicated, may hold values from -0.09375 to 0.09375
- forget_bias: float32 [32], replicated, may hold values from -2 to 2
- keys_cache: bfloat16 [16, 4096, 2048], P(None, 'kv', 'tp'), may hold values from -900 to 900
- values_cache: bfloat16 [16, 4096, 2048], P(None, 'kv', 'tp'), may hold values from -6 to 6
- gates_cache: float32 [16, 32, 4096], P(None, 'tp', 'kv'), as said below
- lengths: int32 [16], replicated, may hold values from 1 to 4096, 32768 in all
- w_out: bfloat16 [2048, 4096], P('tp', 'kv'), may hold values from -0.1875 to 0.1875
- gain_mixer: bfloat16 [4096], replicated, may hold values from 0.099609375 to 1.8984375
- w_up: bfloat16 [4096, 16384], P('kv', 'tp'), may hold values from -0.09375 to 0.09375
- w_down: bfloat16 [16384, 4096], P('tp', 'kv'), may hold values from -0.0625 to 0.0625
Outputs:
- output: bfloat16 [16, 4096], P(None, ('kv', 'tp'))
Inputs may be any that keep to these rules, and one draw needn't show every extreme that they name: One sequence has all 4096 positions live; the lengths add up to half of 16 times 4096. `gates_cache`: along positions each entry is the running sum of per-position log forget gates up to and including that position, so the values never rise.
All inputs are finite; a program needn't handle non-finite values.
Results may differ from a plain program's by a relative error of at most 0.017.
Values may be sent and summed in bfloat16 or wider, within the bound.
A program may use at most 128 MiB of HBM per device.

v0:
```python
import jax
import jax.numpy as jnp
from jax import lax
from jax.sharding import PartitionSpec as P

norm_eps = 1e-06


def combined_all(value, axis, join):
    pieces = jax.tree.map(lambda part: lax.all_gather(part, axis), value)
    head = jax.tree.map(lambda part: part[0], pieces)
    tail = jax.tree.map(lambda part: part[1:], pieces)
    total, _ = lax.scan(lambda total, section: (join(total, section), None), head, tail)
    return total


def combine_parts(earlier, later):
    top = jnp.maximum(earlier[0], later[0])
    early_factor = jnp.exp(earlier[0] - top)
    late_factor = jnp.exp(later[0] - top)
    totals = earlier[1] * early_factor + later[1] * late_factor
    summed = earlier[2] * early_factor[..., None] + later[2] * late_factor[..., None]
    return (top, totals, summed, earlier[3] + later[3])


def channel_mix(residual, gain_mixer, w_up, w_down, kv_index):
    width = gain_mixer.shape[0]
    block_start = kv_index * w_up.shape[0]
    piece = lax.all_gather(residual, "tp", axis=1, tiled=True)
    piece_f = piece.astype(jnp.float32)
    gain_part = lax.dynamic_slice_in_dim(gain_mixer, block_start, piece.shape[1], 0).astype(
        jnp.float32
    )
    scaled = (piece_f * gain_part).astype(jnp.bfloat16)
    upward = jnp.dot(scaled, w_up, preferred_element_type=jnp.float32)
    upward, squares = (upward, jnp.sum(piece_f * piece_f, axis=-1))
    up_total, square_total = lax.psum((upward, squares), "kv")
    mixer_scale = lax.rsqrt(square_total / width + norm_eps)
    active = jax.nn.relu(mixer_scale[:, None] * up_total)
    hidden = (active * active).astype(jnp.bfloat16)
    down = jnp.dot(hidden, w_down, preferred_element_type=jnp.float32)
    return lax.psum_scatter(down, "tp", scatter_dimension=1, tiled=True)


def shards(
    tokens,
    gain_attn,
    w_query,
    w_key,
    w_value,
    w_forget,
    forget_bias,
    keys_cache,
    values_cache,
    gates_cache,
    lengths,
    w_out,
    gain_mixer,
    w_up,
    w_down,
):
    kv_index = lax.axis_index("kv")
    tp_index = lax.axis_index("tp")
    row_block = w_query.shape[0]
    heads_here = gates_cache.shape[1]
    width = gain_attn.shape[0]
    row_start = kv_index * row_block
    head_start = tp_index * heads_here
    block_raw = lax.all_gather(tokens, "tp", axis=1, tiled=True)
    block_f = block_raw.astype(jnp.float32)
    gain_block = lax.dynamic_slice_in_dim(gain_attn, row_start, row_block, 0).astype(jnp.float32)
    block = (block_f * gain_block).astype(jnp.bfloat16)
    forget_block = lax.dynamic_slice(w_forget, (row_start, head_start), (row_block, heads_here))
    part_query = jnp.dot(block, w_query, preferred_element_type=jnp.float32)
    part_key = jnp.dot(block, w_key, preferred_element_type=jnp.float32)
    part_value = jnp.dot(block, w_value, preferred_element_type=jnp.float32)
    part_gate = jnp.dot(block, forget_block, preferred_element_type=jnp.float32)
    part_squares = jnp.sum(block_f * block_f, axis=-1)
    sum_query, sum_key, sum_value, sum_gate, squares = lax.psum(
        (part_query, part_key, part_value, part_gate, part_squares), "kv"
    )
    attn_scale = lax.rsqrt(squares / width + norm_eps)[:, None]
    gate_logit = attn_scale * sum_gate
    query = (attn_scale * sum_query).astype(jnp.bfloat16)
    new_key = (attn_scale * sum_key).astype(jnp.bfloat16)
    new_value = (attn_scale * sum_value).astype(jnp.bfloat16)
    bias_here = lax.dynamic_slice_in_dim(forget_bias, head_start, heads_here, 0)
    forget_log = jax.nn.log_sigmoid(gate_logit + bias_here)
    seqs = tokens.shape[0]
    positions_here = keys_cache.shape[1]
    query_heads = query.reshape(seqs, heads_here, -1)
    head_size = query_heads.shape[-1]
    keys_heads = keys_cache.reshape(seqs, positions_here, heads_here, head_size)
    values_heads = values_cache.reshape(seqs, positions_here, heads_here, head_size)
    scores = jnp.einsum(
        "bhd,bphd->bhp", query_heads, keys_heads, preferred_element_type=jnp.float32
    )
    logits = scores * head_size ** (-0.5) - gates_cache
    positions = kv_index * positions_here + jnp.arange(positions_here, dtype=jnp.int32)
    valid = (positions[None, :] < lengths[:, None])[:, None, :]
    local_top = jnp.max(jnp.where(valid, logits, -1e30), axis=-1)
    weights = jnp.where(valid, jnp.exp(logits - local_top[..., None]), 0.0)
    local_total = jnp.sum(weights, axis=-1)
    local_sum = jnp.einsum(
        "bhp,bphd->bhd",
        weights.astype(jnp.bfloat16),
        values_heads,
        preferred_element_type=jnp.float32,
    )
    at_last = (positions[None, :] == lengths[:, None] - 1)[:, None, :]
    last_local = jnp.sum(jnp.where(at_last, gates_cache, 0.0), axis=-1)
    top, totals, summed, last_gate = combined_all(
        (local_top, local_total, local_sum, last_local), "kv", combine_parts
    )
    top = top + last_gate + forget_log
    own = jnp.sum(
        query_heads.astype(jnp.float32) * new_key.reshape(seqs, heads_here, -1).astype(jnp.float32),
        axis=-1,
    ) * head_size ** (-0.5)
    overall = jnp.maximum(top, own)
    cache_factor = jnp.exp(top - overall)
    own_weight = jnp.exp(own - overall)
    denominator = totals * cache_factor + own_weight
    numerator = summed * cache_factor[..., None] + own_weight[..., None] * new_value.reshape(
        seqs, heads_here, -1
    ).astype(jnp.float32)
    mixed = (numerator / denominator[..., None]).astype(jnp.bfloat16).reshape(seqs, -1)
    partial_value = jnp.dot(mixed, w_out, preferred_element_type=jnp.float32).astype(jnp.bfloat16)
    attended = lax.psum_scatter(partial_value, "tp", scatter_dimension=1, tiled=True).astype(
        jnp.float32
    )
    residual = (tokens.astype(jnp.float32) + attended).astype(jnp.bfloat16)
    mixer = channel_mix(residual, gain_mixer, w_up, w_down, kv_index)
    return (residual.astype(jnp.float32) + mixer).astype(jnp.bfloat16)


def solution(mesh):
    return jax.shard_map(
        shards,
        mesh=mesh,
        in_specs=(
            P(None, ("kv", "tp")),
            P(),
            P("kv", "tp"),
            P("kv", "tp"),
            P("kv", "tp"),
            P(),
            P(),
            P(None, "kv", "tp"),
            P(None, "kv", "tp"),
            P(None, "tp", "kv"),
            P(),
            P("tp", "kv"),
            P(),
            P("kv", "tp"),
            P("tp", "kv"),
        ),
        out_specs=P(None, ("kv", "tp")),
        check_vma=False,
    )
```

profile of v0, /device:TPU:0, one launch (start us, length us, event | category | flops | bytes accessed | tf_op | source)
XLA Modules:
  0.0 361.5 jit_solution(17292253141642095304)
XLA Ops:
  6.5 6.5 %all_gather.30 = bf16[16,512]{1,0:T(8,128)(2,1)S(1)} all-gather(bf16[16,128]{1,0:T(8,128)(2,1)} %param.17), channel_id=1, replica_groups=mesh['kv'=8,'tp'=4] {'tp'}, dimensions={1}, use_global_device_ids=true | all-gather | bytes 20480 | tf_op jit(solution)/shard_map/all_gather | solution.py:69
  15.2 1.8 fusion.28
  17.1 1.8 fusion.23
  18.9 1.4 fusion.21
  21.8 12.3 %copy.32 = bf16[16,512,512]{1,2,0:T(8,128)(2,1)} copy(bf16[16,512,512]{2,1,0:T(8,128)(2,1)} %param.24) | data formatting | bytes 16777216 | tf_op args[7]
  34.1 12.3 %copy.35 = bf16[16,512,512]{1,2,0:T(8,128)(2,1)} copy(bf16[16,512,512]{2,1,0:T(8,128)(2,1)} %param.25) | data formatting | bytes 16777216 | tf_op args[8]
  46.5 46.6 %all-reduce.6.cloned.1.call-done = (f32[16,512]{1,0:T(8,128)}, f32[16]{0:T(128)}, f32[16,512]{1,0:T(8,128)}, f32[16,8]{0,1:T(8,128)}, f32[16,512]{1,0:T(8,128)}) async-done(((f32[16,512]{1,0:T(8,128)}, f32[16]{0:T(128)}, f32[16,512]{1,0:T(8,128)}, f32[16,8]{0,1:T(8,128)}, f32[16,512]{1,0:T(8,128)}), (f32[16,512]{1,0:T(8,128)}, f32[16]{0:T(128)}, f32[16,512]{1,0:T(8,128)}, f32[16,8]{0,1:T(8,128)}, ...) | async-done | bytes 98896 | tf_op jit(solution)/shard_map/psum | solution.py:79
  93.8 0.9 fusion.16
  94.8 4.7 %fusion.38 = f32[16,8,1,512]{3,2,1,0:T(1,128)S(1)} fusion(bf16[16,8,64,1]{2,3,1,0:T(2,128)(2,1)S(1)} %reshape.122, bf16[16,512,8,64]{1,3,2,0:T(8,128)(2,1)} %bitcast.59), kind=kOutput, calls=%fused_computation.68 | convolution fusion | flops 8388608 | bytes 8667136 | tf_op jit(solution)/shard_map/bhd,bphd->bhp/dot_general | solution.py:95
  100.6 2.3 fusion.4
  102.8 31.3 %all-gather.2 = f32[128,8,64]{2,1,0:T(8,128)S(1)} all-gather(f32[16,8,64]{2,1,0:T(8,128)S(1)} %bitcast.65), channel_id=4, replica_groups=mesh['kv'=8,'tp'=4] {'kv'}, dimensions={0}, use_global_device_ids=true | all-gather | bytes 294912 | tf_op jit(solution)/shard_map/all_gather | solution.py:10
  134.2 30.6 %all-gather.6 = f32[8,16,8]{1,2,0:T(8,128)S(1)} all-gather(f32[1,16,8]{1,2,0:T(8,128)S(1)} %bitcast.67), channel_id=5, replica_groups=mesh['kv'=8,'tp'=4] {'kv'}, dimensions={0}, use_global_device_ids=true | all-gather | bytes 4608 | tf_op jit(solution)/shard_map/all_gather | solution.py:10
  164.9 30.6 %all-gather.5 = f32[8,16,8]{1,2,0:T(8,128)S(1)} all-gather(f32[1,16,8]{1,2,0:T(8,128)S(1)} %bitcast.68), channel_id=3, replica_groups=mesh['kv'=8,'tp'=4] {'kv'}, dimensions={0}, use_global_device_ids=true | all-gather | bytes 4608 | tf_op jit(solution)/shard_map/all_gather | solution.py:10
  195.6 30.6 %all-gather.4 = f32[8,16,8]{1,2,0:T(8,128)S(1)} all-gather(f32[1,16,8]{1,2,0:T(8,128)S(1)} %bitcast.69), channel_id=2, replica_groups=mesh['kv'=8,'tp'=4] {'kv'}, dimensions={0}, use_global_device_ids=true | all-gather | bytes 4608 | tf_op jit(solution)/shard_map/all_gather | solution.py:10
  226.3 2.1 while.16
  231.1 19.4 %reduce-scatter.7.cloned.1.call-done = bf16[128,16]{1,0:T(8,128)(2,1)} async-done(((bf16[512,16]{1,0:T(8,128)(2,1)}), bf16[128,16]{1,0:T(8,128)(2,1)}) %reduce-scatter.7.cloned.1.call-update) | async-done | bytes 4112
  250.5 0.8 copy.46
  251.3 5.2 %all_gather.39 = bf16[16,512]{1,0:T(8,128)(2,1)S(1)} all-gather(bf16[16,128]{1,0:T(8,128)(2,1)S(1)} %add_convert_fusion.1), channel_id=1, replica_groups=mesh['kv'=8,'tp'=4] {'tp'}, dimensions={1}, use_global_device_ids=true | all-gather | bytes 20480 | tf_op jit(solution)/shard_map/all_gather | solution.py:29
  256.5 3.5 fusion.18
  260.2 21.4 %psum.54 = f32[16]{0:T(128)S(1)} all-reduce(f32[16]{0:T(128)S(1)} %fusion.14), channel_id=1, replica_groups=mesh['kv'=8,'tp'=4] {'kv'}, use_global_device_ids=true, to_apply=%region_14.15 | all-reduce | flops 16 | bytes 128 | tf_op jit(solution)/shard_map/psum | solution.py:37
  281.6 49.6 %all-reduce.4.cloned.1.call-done = f32[16,4096]{1,0:T(8,128)} async-done(((f32[16,4096]{1,0:T(8,128)}), f32[16,4096]{1,0:T(8,128)}) %all-reduce.4.cloned.1.call-update) | async-done | bytes 262160 | tf_op jit(solution)/shard_map/psum | solution.py:37
  331.2 3.6 fusion.9
  334.8 18.9 %reduce-scatter.5.cloned.1.call-done = f32[16,128]{1,0:T(8,128)} async-done(((f32[16,512]{1,0:T(8,128)}), f32[16,128]{1,0:T(8,128)}) %reduce-scatter.5.cloned.1.call-update) | async-done | bytes 8208 | tf_op jit(solution)/shard_map/reduce_scatter | solution.py:42
  353.7 1.3 add_convert_fusion
  (92 shorter events, 10.7 us)
Async XLA Ops:
  6.5 7.9 %copy-start = (bf16[512,512]{1,0:T(8,128)(2,1)S(1)}, bf16[512,512]{1,0:T(8,128)(2,1)}, u32[]{:S(2)}) copy-start(bf16[512,512]{1,0:T(8,128)(2,1)} %param.20) | copy-start | bytes 1572868
  6.5 86.6 %all-reduce.6.cloned.1.call-start = ((), (), s32[]{:S(2)}) async-start(), calls=%async_computation.5 | async-start | bytes 205824 | tf_op jit(solution)/shard_map/psum | solution.py:79
  20.3 230.1 %reduce-scatter.7.cloned.1.call-start = ((), (), s32[]{:S(2)}) async-start(), calls=%async_computation.4 | async-start | bytes 163840
  34.1 12.3 %copy-start.5 = (f32[32]{0:T(128)S(1)}, f32[32]{0:T(128)}, u32[]{:S(2)}) copy-start(f32[32]{0:T(128)} %param.23) | copy-start | bytes 388
  46.4 53.1 %copy-start.1 = (f32[16,8,512]{2,1,0:T(8,128)S(1)}, f32[16,8,512]{2,1,0:T(8,128)}, u32[]{:S(2)}) copy-start(f32[16,8,512]{2,1,0:T(8,128)} %param.26) | copy-start | bytes 786436
  94.7 5.1 %slice-start = ((s8[8388608]{0:T(1024)(128)(4,1)}), s8[4194304]{0:T(1024)(128)(4,1)S(1)}, s32[]{:S(2)}) async-start(s8[8388608]{0:T(1024)(128)(4,1)} %bitcast.60), calls=%async_computation.6 | async-start | bytes 8388608
  94.7 5.8 %slice-start.1 = ((s8[8388608]{0:T(1024)(128)(4,1)}), s8[4194304]{0:T(1024)(128)(4,1)S(1)}, s32[]{:S(2)}) async-start(s8[8388608]{0:T(1024)(128)(4,1)} %bitcast.60), calls=%async_computation.7 | async-start | bytes 8388608
  99.5 129.2 %copy-start.4 = (f32[16,8]{0,1:T(8,128)S(1)}, f32[16,8]{0,1:T(8,128)}, u32[]{:S(2)}) copy-start(f32[16,8]{0,1:T(8,128)} %get-tuple-element.82) | copy-start | bytes 1540
  99.5 129.8 %copy-start.2 = (bf16[512,512]{1,0:T(8,128)(2,1)S(1)}, bf16[512,512]{1,0:T(8,128)(2,1)}, u32[]{:S(2)}) copy-start(bf16[512,512]{1,0:T(8,128)(2,1)} %param.28) | copy-start | bytes 1572868
  99.5 151.8 %copy-start.3 = (bf16[16,128]{1,0:T(8,128)(2,1)S(1)}, bf16[16,128]{1,0:T(8,128)(2,1)}, u32[]{:S(2)}) copy-start(bf16[16,128]{1,0:T(8,128)(2,1)} %param.17) | copy-start | bytes 12292
  230.2 101.0 %all-reduce.4.cloned.1.call-start = ((), (), s32[]{:S(2)}) async-start(), calls=%async_computation.2 | async-start | bytes 524288 | tf_op jit(solution)/shard_map/psum | solution.py:37
  260.1 93.7 %reduce-scatter.5.cloned.1.call-start = ((), (), s32[]{:S(2)}) async-start(), calls=%async_computation.3 | async-start | bytes 40960 | tf_op jit(solution)/shard_map/reduce_scatter | solution.py:42
Sparse Core Ops, SparseCore 0:
  20.4 72.6 all-reduce.5
  230.4 20.0 reduce-scatter.6
  260.2 71.0 all-reduce.3
  335.0 18.6 reduce-scatter.4
where the time goes:
time: 363 us; the launch traced here: 362 us
  blocking collectives  156 us (43%)
  waiting for transfers between devices  135 us (37%)
  local copies, waits for them, and re-layouts  29.1 us (8%)
  matrix products  20.1 us (6%)
  between operations  13.3 us (4%)
  other arithmetic  8.07 us (2%)
    all_gather x4, blocking collectives, combined_all(): pieces = jax.tree.map(lambda part: lax.all_gather(part, axis), value)  123 us
    psum x1, waiting for transfers between devices, channel_mix(): up_total, square_total = lax.psum((upward, squares), 'kv')  49.6 us
    psum x1, waiting for transfers between devices, shards(): lax.psum((part_query, part_key, part_value, part_gate, part_squares), 'kv')  46.6 us
    unnamed x20, local copies, waits for them, and re-layouts  27 us
    psum x1, blocking collectives, channel_mix(): up_total, square_total = lax.psum((upward, squares), 'kv')  21.4 us
    unnamed x5, waiting for transfers between devices  19.5 us
    reduce_scatter x1, waiting for transfers between devices, channel_mix(): return lax.psum_scatter(down, 'tp', scatter_dimension=1, tiled=True)  18.9 us
  transfers between devices with their start and end apart: 4, of which 4 were waited for; matrix products, arithmetic and copies ran while one was open for 7% of the time, Pallas kernels for 0%

commit v1 on v0

--- a/solution.py
+++ b/solution.py
@@ -1,6 +1,10 @@
+import functools
+
 import jax
 import jax.numpy as jnp
 from jax import lax
+from jax.experimental import pallas as pl
+from jax.experimental.pallas import tpu as pltpu
 from jax.sharding import PartitionSpec as P
 
 norm_eps = 1e-06
@@ -134,9 +138,512 @@
     return (residual.astype(jnp.float32) + mixer).astype(jnp.bfloat16)
 
 
+f32, bf16 = jnp.float32, jnp.bfloat16
+LANES = 128
+
+
+def split_squares(values):
+    total = jnp.sum(values * values, axis=-1, keepdims=True)
+    high = total.astype(bf16).astype(f32)
+    lane = lax.broadcasted_iota(jnp.int32, (values.shape[0], LANES), 1)
+    return jnp.where(lane == 0, high, jnp.where(lane == 1, total - high, 0.0))
+
+
+def joined_squares(block):
+    return jnp.sum(block, axis=-1, keepdims=True)
+
+
+def fused(
+    n_kv,
+    n_tp,
+    tokens,
+    gain_attn,
+    forget_bias,
+    lengths,
+    gain_mixer,
+    w_query,
+    w_key,
+    w_value,
+    w_forget,
+    keys_cache,
+    values_cache,
+    gates_cache,
+    w_out,
+    w_up,
+    w_down,
+    out,
+    wq,
+    wk,
+    wv,
+    wf,
+    keys,
+    values,
+    gates,
+    wo,
+    wu,
+    wd,
+    tok_all,
+    q_send,
+    q_all,
+    p_send,
+    p_all,
+    a_send,
+    a_all,
+    m_send,
+    m_all,
+    o_send,
+    o_all,
+    u_send,
+    u_all,
+    h_send,
+    h_all,
+    f_send,
+    f_all,
+    query,
+    mix,
+    res,
+    load_sem,
+    kv_out,
+    kv_in,
+    tp_out,
+    tp_in,
+):
+    kv, tp = lax.axis_index("kv"), lax.axis_index("tp")
+    seqs, piece = tokens.shape
+    rows, cols = wq.shape
+    positions = keys.shape[1]
+    heads = gates.shape[1]
+    all_heads = wf.shape[1]
+    size = cols // heads
+    mine = seqs // n_kv
+    width = gain_attn.shape[1]
+    unit = wu.shape[1] // n_kv
+
+    row_at = pl.multiple_of(kv * rows, rows)
+    sources = [
+        (w_query, wq),
+        (w_key, wk),
+        (w_value, wv),
+        (w_forget.at[pl.ds(row_at, rows), :], wf),
+        (keys_cache, keys),
+        (gates_cache, gates),
+        (values_cache, values),
+        (w_out, wo),
+        (w_up, wu),
+        (w_down, wd),
+    ]
+    loads = [pltpu.make_async_copy(a, b, load_sem.at[i]) for i, (a, b) in enumerate(sources)]
+    for load in loads:
+        load.start()
+    ld_q, ld_k, ld_v, ld_f, ld_keys, ld_gates, ld_values, ld_o, ld_u, ld_d = loads
+
+    barrier = pltpu.get_barrier_semaphore()
+    for j in range(1, n_kv):
+        pl.semaphore_signal(
+            barrier,
+            inc=1,
+            device_id=(lax.rem(kv + j, n_kv), tp),
+            device_id_type=pl.DeviceIdType.MESH,
+        )
+    for j in range(1, n_tp):
+        pl.semaphore_signal(
+            barrier,
+            inc=1,
+            device_id=(kv, lax.rem(tp + j, n_tp)),
+            device_id_type=pl.DeviceIdType.MESH,
+        )
+    pl.semaphore_wait(barrier, n_kv + n_tp - 2)
+
+    def over_kv(phase, j, source, landing):
+        peer = lax.rem(kv + j, n_kv)
+        return pltpu.make_async_remote_copy(
+            src_ref=source(peer),
+            dst_ref=landing.at[kv],
+            send_sem=kv_out.at[phase, j],
+            recv_sem=kv_in.at[phase, kv],
+            device_id=(peer, tp),
+            device_id_type=pl.DeviceIdType.MESH,
+        )
+
+    def from_kv(phase, j, source, landing):
+        peer = lax.rem(kv + n_kv - j, n_kv)
+        pltpu.make_async_remote_copy(
+            src_ref=source(peer),
+            dst_ref=landing.at[peer],
+            send_sem=kv_out.at[phase, j],
+            recv_sem=kv_in.at[phase, peer],
+            device_id=(peer, tp),
+            device_id_type=pl.DeviceIdType.MESH,
+        ).wait_recv()
+        return peer
+
+    def over_tp(phase, j, source, landing):
+        peer = lax.rem(tp + j, n_tp)
+        return pltpu.make_async_remote_copy(
+            src_ref=source(peer),
+            dst_ref=landing.at[tp],
+            send_sem=tp_out.at[phase, j],
+            recv_sem=tp_in.at[phase, tp],
+            device_id=(kv, peer),
+            device_id_type=pl.DeviceIdType.MESH,
+        )
+
+    def from_tp(phase, j, source, landing):
+        peer = lax.rem(tp + n_tp - j, n_tp)
+        pltpu.make_async_remote_copy(
+            src_ref=source(peer),
+            dst_ref=landing.at[peer],
+            send_sem=tp_out.at[phase, j],
+            recv_sem=tp_in.at[phase, peer],
+            device_id=(kv, peer),
+            device_id_type=pl.DeviceIdType.MESH,
+        ).wait_recv()
+        return peer
+
+    pending = []
+
+    def send_kv(phase, j, source, landing):
+        copy = over_kv(phase, j, source, landing)
+        copy.start()
+        pending.append(copy)
+
+    def send_tp(phase, j, source, landing):
+        copy = over_tp(phase, j, source, landing)
+        copy.start()
+        pending.append(copy)
+
+    for j in range(1, n_tp):
+        send_tp(0, j, lambda peer: tokens, tok_all)
+    tok_all[tp] = tokens[...]
+    gain_a = gain_attn[:, pl.ds(row_at, rows)].astype(f32)
+    gain_m = gain_mixer[:, pl.ds(row_at, rows)].astype(f32)
+    for j in range(1, n_tp):
+        from_tp(0, j, lambda peer: tokens, tok_all)
+    tok = jnp.concatenate([tok_all[t] for t in range(n_tp)], axis=1).astype(f32)
+    scaled = (tok * gain_a).astype(bf16)
+
+    ld_q.wait()
+    squares = split_squares(tok)
+    q_send[:, :cols] = jnp.dot(scaled, wq[...], preferred_element_type=f32).astype(bf16)
+    q_send[:, cols:] = squares.astype(bf16)
+    for j in range(1, n_kv):
+        send_kv(0, j, lambda peer: q_send, q_all)
+    q_all[kv] = q_send[...]
+
+    ld_k.wait()
+    ld_v.wait()
+    ld_f.wait()
+    part_key = jnp.dot(scaled, wk[...], preferred_element_type=f32)
+    part_value = jnp.dot(scaled, wv[...], preferred_element_type=f32)
+    part_gate = jnp.dot(scaled, wf[...], preferred_element_type=f32)
+    for o in range(n_kv):
+        at = slice(o * mine, (o + 1) * mine)
+        p_send[o, :, :cols] = part_key[at]
+        p_send[o, :, cols : 2 * cols] = part_value[at]
+        p_send[o, :, 2 * cols : 2 * cols + all_heads] = part_gate[at]
+        p_send[o, :, 2 * cols + all_heads :] = jnp.zeros((mine, LANES - all_heads), f32)
+    for j in range(1, n_kv):
+        send_kv(1, j, lambda peer: p_send.at[peer], p_all)
+    p_all[kv] = p_send[kv]
+
+    for j in range(1, n_kv):
+        from_kv(0, j, lambda peer: q_send, q_all)
+    q_total = q_all[0].astype(f32)
+    for o in range(1, n_kv):
+        q_total = q_total + q_all[o].astype(f32)
+    attn_scale = lax.rsqrt(joined_squares(q_total[:, cols:]) / width + norm_eps)
+    query[:, :cols] = (attn_scale * q_total[:, :cols]).astype(bf16).astype(f32)
+    query[:, cols:] = jnp.broadcast_to(attn_scale, (seqs, LANES))
+
+    ld_keys.wait()
+    ld_gates.wait()
+    ld_values.wait()
+    head_row = lax.broadcasted_iota(jnp.int32, (heads, cols), 0)
+    own_block = head_row == lax.broadcasted_iota(jnp.int32, (heads, cols), 1) // size
+    place = kv * positions + lax.broadcasted_iota(jnp.int32, (heads, positions), 1)
+    stat_row = lax.broadcasted_iota(jnp.int32, (heads, LANES), 0)
+    stat_lane = lax.broadcasted_iota(jnp.int32, (heads, LANES), 1)
+
+    def attend(owner):
+        for r in range(mine):
+            b = owner * mine + r
+            spread = jnp.where(own_block, query[pl.ds(b, 1), :cols], 0.0).astype(bf16)
+            scores = lax.dot_general(
+                spread, keys[b], (((1,), (1,)), ((), ())), preferred_element_type=f32
+            )
+            gate = gates[b]
+            length = lengths[b]
+            valid = place < length
+            logits = scores * size ** (-0.5) - gate
+            top = jnp.max(jnp.where(valid, logits, -1e30), axis=-1, keepdims=True)
+            weights = jnp.where(valid, jnp.exp(logits - top), 0.0)
+            total = jnp.sum(weights, axis=-1, keepdims=True)
+            last = jnp.sum(jnp.where(place == length - 1, gate, 0.0), axis=-1, keepdims=True)
+            summed = jnp.dot(weights.astype(bf16), values[b], preferred_element_type=f32)
+            a_send[owner, r : r + 1, :cols] = jnp.sum(
+                jnp.where(own_block, summed, 0.0), axis=0, keepdims=True
+            )
+            stats = jnp.where(
+                stat_lane == stat_row,
+                top,
+                jnp.where(
+                    stat_lane == stat_row + heads,
+                    total,
+                    jnp.where(stat_lane == stat_row + 2 * heads, last, 0.0),
+                ),
+            )
+            a_send[owner, r : r + 1, cols:] = jnp.sum(stats, axis=0, keepdims=True)
+
+    def attend_for(j, carry):
+        attend(lax.rem(kv + j, n_kv))
+        over_kv(2, j, lambda peer: a_send.at[peer], a_all).start()
+        return carry
+
+    lax.fori_loop(1, n_kv, attend_for, 0)
+    attend(kv)
+    a_all[kv] = a_send[kv]
+
+    for j in range(1, n_kv):
+        from_kv(1, j, lambda peer: p_send.at[peer], p_all)
+    p_total = p_all[0]
+    for o in range(1, n_kv):
+        p_total = p_total + p_all[o]
+    own_rows = [query[pl.ds(kv * mine + r, 1), :] for r in range(mine)]
+    own_query = jnp.concatenate(own_rows, axis=0)
+    own_scale = own_query[:, cols : cols + 1]
+    own_query = own_query[:, :cols]
+    new_key = (own_scale * p_total[:, :cols]).astype(bf16).astype(f32)
+    new_value = (own_scale * p_total[:, cols : 2 * cols]).astype(bf16).astype(f32)
+    gate_logit = own_scale * p_total[:, 2 * cols : 2 * cols + all_heads] + forget_bias[...]
+    forget_log = jnp.minimum(gate_logit, 0.0) - jnp.log1p(jnp.exp(-jnp.abs(gate_logit)))
+    col_head = lax.broadcasted_iota(jnp.int32, (mine, cols), 1) // size
+    forget_wide = jnp.zeros((mine, cols), f32)
+    for h in range(all_heads):
+        forget_wide = jnp.where(col_head + tp * heads == h, forget_log[:, h : h + 1], forget_wide)
+    product = own_query * new_key
+    own = jnp.zeros((mine, cols), f32)
+    for h in range(heads):
+        inside = col_head == h
+        own = jnp.where(
+            inside, jnp.sum(jnp.where(inside, product, 0.0), axis=-1, keepdims=True), own
+        )
+    own = own * size ** (-0.5)
+
+    for j in range(1, n_kv):
+        from_kv(2, j, lambda peer: a_send.at[peer], a_all)
+
+    def wide(part, first):
+        result = jnp.zeros((mine, cols), f32)
+        for h in range(heads):
+            result = jnp.where(col_head == h, part[:, first + h : first + h + 1], result)
+        return result
+
+    tops = [wide(a_all[o, :, cols:], 0) for o in range(n_kv)]
+    top = functools.reduce(jnp.maximum, tops)
+    totals = jnp.zeros((mine, cols), f32)
+    summed = jnp.zeros((mine, cols), f32)
+    stat_sum = a_all[0, :, cols:]
+    for o in range(1, n_kv):
+        stat_sum = stat_sum + a_all[o, :, cols:]
+    for o in range(n_kv):
+        factor = jnp.exp(tops[o] - top)
+        totals = totals + factor * wide(a_all[o, :, cols:], heads)
+        summed = summed + factor * a_all[o, :, :cols]
+    top = top + wide(stat_sum, 2 * heads) + forget_wide
+    overall = jnp.maximum(top, own)
+    cache_factor = jnp.exp(top - overall)
+    own_weight = jnp.exp(own - overall)
+    denominator = totals * cache_factor + own_weight
+    numerator = summed * cache_factor + own_weight * new_value
+    m_send[...] = (numerator / denominator).astype(bf16).astype(f32)
+    for j in range(1, n_kv):
+        send_kv(3, j, lambda peer: m_send, m_all)
+    m_all[kv] = m_send[...]
+    ld_o.wait()
+    for j in range(1, n_kv):
+        from_kv(3, j, lambda peer: m_send, m_all)
+    for o in range(n_kv):
+        mix[o * mine : (o + 1) * mine, :] = m_all[o]
+
+    o_send[...] = jnp.dot(mix[...].astype(bf16), wo[...], preferred_element_type=f32).astype(bf16)
+    for j in range(1, n_tp):
+        send_tp(1, j, lambda peer: o_send, o_all)
+    o_all[tp] = o_send[...]
+    ld_u.wait()
+    for j in range(1, n_tp):
+        from_tp(1, j, lambda peer: o_send, o_all)
+    attended = o_all[0].astype(f32)
+    for t in range(1, n_tp):
+        attended = attended + o_all[t].astype(f32)
+    residual = (tok + attended).astype(bf16).astype(f32)
+    for t in range(n_tp):
+        res[t] = residual[:, t * piece : (t + 1) * piece]
+
+    scaled_mid = (residual * gain_m).astype(bf16)
+    squares_mid = split_squares(residual).astype(bf16)
+
+    def up_piece(owner):
+        at = pl.multiple_of(owner * unit, unit)
+        u_send[owner, :, :unit] = jnp.dot(
+            scaled_mid, wu[:, pl.ds(at, unit)], preferred_element_type=f32
+        ).astype(bf16)
+        u_send[owner, :, unit:] = squares_mid
+
+    for j in range(1, n_kv):
+        up_piece(lax.rem(kv + j, n_kv))
+        send_kv(4, j, lambda peer: u_send.at[peer], u_all)
+    up_piece(kv)
+    u_all[kv] = u_send[kv]
+    for j in range(1, n_kv):
+        from_kv(4, j, lambda peer: u_send.at[peer], u_all)
+    up_total = u_all[0].astype(f32)
+    for o in range(1, n_kv):
+        up_total = up_total + u_all[o].astype(f32)
+    mixer_scale = lax.rsqrt(joined_squares(up_total[:, unit:]) / width + norm_eps)
+    active = jnp.maximum(mixer_scale * up_total[:, :unit], 0.0)
+    h_send[...] = (active * active).astype(bf16)
+    for j in range(1, n_kv):
+        send_kv(5, j, lambda peer: h_send, h_all)
+
+    ld_d.wait()
+
+    def down_piece(block, owner):
+        at = pl.multiple_of(owner * unit, unit)
+        return jnp.dot(block, wd[pl.ds(at, unit), :], preferred_element_type=f32)
+
+    down = down_piece(h_send[...], kv)
+    for j in range(1, n_kv):
+        peer = from_kv(5, j, lambda peer: h_send, h_all)
+        down = down + down_piece(h_all[peer], peer)
+    for t in range(n_tp):
+        f_send[t] = down[:, t * piece : (t + 1) * piece]
+    for j in range(1, n_tp):
+        send_tp(2, j, lambda peer: f_send.at[peer], f_all)
+    f_all[tp] = f_send[tp]
+    for j in range(1, n_tp):
+        from_tp(2, j, lambda peer: f_send.at[peer], f_all)
+    mixer = f_all[0]
+    for t in range(1, n_tp):
+        mixer = mixer + f_all[t]
+    out[...] = (res[tp] + mixer).astype(bf16)
+
+    for copy in pending:
+        copy.wait_send()
+    for j in range(1, n_kv):
+        over_kv(2, j, lambda peer: a_send.at[peer], a_all).wait_send()
+
+
+def layer(n_kv, n_tp, *arrays):
+    (
+        tokens,
+        gain_attn,
+        w_query,
+        w_key,
+        w_value,
+        w_forget,
+        forget_bias,
+        keys_cache,
+        values_cache,
+        gates_cache,
+        lengths,
+        w_out,
+        gain_mixer,
+        w_up,
+        w_down,
+    ) = arrays
+    seqs, piece = tokens.shape
+    rows, cols = w_query.shape
+    heads = gates_cache.shape[1]
+    all_heads = w_forget.shape[1]
+    unit = w_up.shape[1] // n_kv
+    fits = (
+        piece % LANES == 0
+        and cols % LANES == 0
+        and unit % LANES == 0
+        and seqs % n_kv == 0
+        and 3 * heads <= LANES
+        and all_heads < LANES
+        and w_out.shape == (cols, rows)
+        and n_kv > 1
+        and n_tp > 1
+    )
+    if not fits:
+        return shards(*arrays)
+    mine = seqs // n_kv
+    vmem = pl.BlockSpec(memory_space=pltpu.VMEM)
+    smem = pl.BlockSpec(memory_space=pltpu.SMEM)
+    anywhere = pl.BlockSpec(memory_space=pl.ANY)
+
+    def like(x):
+        return pltpu.VMEM(x.shape, x.dtype)
+
+    return pl.pallas_call(
+        functools.partial(fused, n_kv, n_tp),
+        out_shape=jax.ShapeDtypeStruct((seqs, piece), bf16),
+        in_specs=[vmem, vmem, vmem, smem, vmem] + [anywhere] * 10,
+        out_specs=vmem,
+        scratch_shapes=[
+            like(w_query),
+            like(w_key),
+            like(w_value),
+            pltpu.VMEM((rows, all_heads), bf16),
+            like(keys_cache),
+            like(values_cache),
+            like(gates_cache),
+            like(w_out),
+            like(w_up),
+            like(w_down),
+            pltpu.VMEM((n_tp, seqs, piece), bf16),
+            pltpu.VMEM((seqs, cols + LANES), bf16),
+            pltpu.VMEM((n_kv, seqs, cols + LANES), bf16),
+            pltpu.VMEM((n_kv, mine, 2 * cols + LANES), f32),
+            pltpu.VMEM((n_kv, mine, 2 * cols + LANES), f32),
+            pltpu.VMEM((n_kv, mine, cols + LANES), f32),
+            pltpu.VMEM((n_kv, mine, cols + LANES), f32),
+            pltpu.VMEM((mine, cols), f32),
+            pltpu.VMEM((n_kv, mine, cols), f32),
+            pltpu.VMEM((seqs, rows), bf16),
+            pltpu.VMEM((n_tp, seqs, rows), bf16),
+            pltpu.VMEM((n_kv, seqs, unit + LANES), bf16),
+            pltpu.VMEM((n_kv, seqs, unit + LANES), bf16),
+            pltpu.VMEM((seqs, unit), bf16),
+            pltpu.VMEM((n_kv, seqs, unit), bf16),
+            pltpu.VMEM((n_tp, seqs, piece), f32),
+            pltpu.VMEM((n_tp, seqs, piece), f32),
+            pltpu.VMEM((seqs, cols + LANES), f32),
+            pltpu.VMEM((seqs, cols), f32),
+            pltpu.VMEM((n_tp, seqs, piece), f32),
+            pltpu.SemaphoreType.DMA((10,)),
+            pltpu.SemaphoreType.DMA((6, n_kv)),
+            pltpu.SemaphoreType.DMA((6, n_kv)),
+            pltpu.SemaphoreType.DMA((3, n_tp)),
+            pltpu.SemaphoreType.DMA((3, n_tp)),
+        ],
+        compiler_params=pltpu.CompilerParams(
+            collective_id=0, has_side_effects=True, vmem_limit_bytes=60 * 1024 * 1024
+        ),
+    )(
+        tokens,
+        gain_attn.reshape(1, -1),
+        forget_bias.reshape(1, -1),
+        lengths,
+        gain_mixer.reshape(1, -1),
+        w_query,
+        w_key,
+        w_value,
+        w_forget,
+        keys_cache,
+        values_cache,
+        gates_cache,
+        w_out,
+        w_up,
+        w_down,
+    )
+
+
 def solution(mesh):
     return jax.shard_map(
-        shards,
+        functools.partial(layer, mesh.shape["kv"], mesh.shape["tp"]),
         mesh=mesh,
         in_specs=(
             P(None, ("kv", "tp")),

time: 363 us -> 54.8 us (0.15)
  blocking collectives: 156 us -> 0 us
  waiting for transfers between devices: 135 us -> 0 us
  Pallas kernels: 0 us -> 48.2 us
  local copies, waits for them, and re-layouts: 29.1 us -> 6.16 us
  matrix products: 20.1 us -> 0 us
  between operations: 13.3 us -> 0.01 us
  other arithmetic: 8.07 us -> 0 us
    all_gather x6 -> x0, blocking collectives: 135 us -> none  [the longest x4 123 us: combined_all(): pieces = jax.tree.map(lambda part: lax.all_gather(part, axis), value)]
    psum x2 -> x0, waiting for transfers between devices: 96.2 us -> none  [the longest x1 49.6 us: channel_mix(): up_total, square_total = lax.psum((upward, squares), 'kv')]
    pallas_call x0 -> x1, Pallas kernels: none -> 48.2 us  [layer(): pl.pallas_call(functools.partial(fused, n_kv, n_tp), out_shape=jax.ShapeD...]
    unnamed x20 -> x2, local copies, waits for them, and re-layouts: 27 us -> 3.55 us
    psum x1 -> x0, blocking collectives: 21.4 us -> none  [channel_mix(): up_total, square_total = lax.psum((upward, squares), 'kv')]
    dot_general x9 -> x0, matrix products: 20.1 us -> none  [the longest x1 4.72 us: shards(): jnp.einsum('bhd,bphd->bhp', query_heads, keys_heads, preferred_element_ty...]
    unnamed x5 -> x0, waiting for transfers between devices: 19.5 us -> none
    reduce_scatter x1 -> x0, waiting for transfers between devices: 18.9 us -> none  [channel_mix(): return lax.psum_scatter(down, 'tp', scatter_dimension=1, tiled=True)]
  transfers between devices with their start and end apart: 4 -> 0, of which waited for: 4 -> 0; matrix products, arithmetic and copies ran while one was open for 7% -> 0% of each run, Pallas kernels for 0% -> 0%
where the time goes in v1:
time: 54.8 us; the launch traced here: 54.3 us
  Pallas kernels  48.2 us (88%)
  local copies, waits for them, and re-layouts  6.16 us (11%)
    pallas_call x1, Pallas kernels, layer(): pl.pallas_call(functools.partial(fused, n_kv, n_tp), out_shape=jax.ShapeD...  48.2 us
    unnamed x2, local copies, waits for them, and re-layouts  3.55 us
    reshape x1, local copies, waits for them, and re-layouts, layer(): gain_attn.reshape(1, -1)  1.3 us
    reshape x1, local copies, waits for them, and re-layouts, layer(): gain_mixer.reshape(1, -1)  1.3 us

profile of v1, /device:TPU:0, one launch (start us, length us, event | category | flops | bytes accessed | tf_op | source)
XLA Modules:
  0.0 54.3 jit_solution(192447206139690074)
XLA Ops:
  0.0 1.3 %reshape.9.gain_attn = bf16[1,4096]{1,0:T(2,128)(2,1)} reshape(bf16[4096]{0:T(1024)(128)(2,1)} %param.16) | data formatting | bytes 16384 | tf_op jit(solution)/shard_map/reshape | solution.py:627
  1.3 1.3 %reshape.11.gain_mixer = bf16[1,4096]{1,0:T(2,128)(2,1)} reshape(bf16[4096]{0:T(1024)(128)(2,1)} %param.27) | data formatting | bytes 16384 | tf_op jit(solution)/shard_map/reshape | solution.py:630
  2.6 2.3 %copy.16.w_forget = bf16[4096,32]{1,0:T(8,128)(2,1)} copy(bf16[4096,32]{0,1:T(8,128)(2,1)} %param.20) | data formatting | bytes 524288 | tf_op args[5]
  4.9 48.2 %shard_map.145 = bf16[16,128]{1,0:T(8,128)(2,1)} custom-call(bf16[16,128]{1,0:T(8,128)(2,1)} %tokens.1, bf16[1,4096]{1,0:T(2,128)(2,1)} %reshape.9.gain_attn, f32[1,32]{1,0:T(1,128)} %bitcast.1, s32[16]{0:T(128)} %lengths.1, bf16[1,4096]{1,0:T(2,128)(2,1)} %reshape.11.gain_mixer, bf16[512,512]{1,0:T(8,128)(2,1)} %w_query.1, bf16[512,512]{1,0:T(8,128)(2,1)} %w_key.1, ...), custom_call_target="tpu_custom_call" | custom-call | tf_op jit(solution)/shard_map/pallas_call | solution.py:580
  53.1 1.3 %copy.18 = bf16[16,128]{1,0:T(8,128)(2,1)} copy(bf16[16,128]{1,0:T(8,128)(2,1)} %shard_map.145) | data formatting | bytes 8192

commit v2 on v1

--- a/solution.py
+++ b/solution.py
@@ -142,15 +142,16 @@
 LANES = 128
 
 
-def split_squares(values):
-    total = jnp.sum(values * values, axis=-1, keepdims=True)
-    high = total.astype(bf16).astype(f32)
-    lane = lax.broadcasted_iota(jnp.int32, (values.shape[0], LANES), 1)
-    return jnp.where(lane == 0, high, jnp.where(lane == 1, total - high, 0.0))
-
-
-def joined_squares(block):
-    return jnp.sum(block, axis=-1, keepdims=True)
+def to_row(column):
+    shape = (column.shape[0], LANES)
+    same = lax.broadcasted_iota(jnp.int32, shape, 0) == lax.broadcasted_iota(jnp.int32, shape, 1)
+    return jnp.sum(jnp.where(same, column, 0.0), axis=0, keepdims=True)
+
+
+def to_column(row, count):
+    shape = (count, LANES)
+    same = lax.broadcasted_iota(jnp.int32, shape, 0) == lax.broadcasted_iota(jnp.int32, shape, 1)
+    return jnp.sum(jnp.where(same, row, 0.0), axis=-1, keepdims=True)
 
 
 def fused(
@@ -202,6 +203,8 @@
     query,
     mix,
     res,
+    s_send,
+    s_all,
     load_sem,
     kv_out,
     kv_in,
@@ -213,10 +216,10 @@
     rows, cols = wq.shape
     positions = keys.shape[1]
     heads = gates.shape[1]
-    all_heads = wf.shape[1]
+    all_heads = wf.shape[0]
     size = cols // heads
     mine = seqs // n_kv
-    width = gain_attn.shape[1]
+    width = gain_attn.shape[0]
     unit = wu.shape[1] // n_kv
 
     row_at = pl.multiple_of(kv * rows, rows)
@@ -224,7 +227,7 @@
         (w_query, wq),
         (w_key, wk),
         (w_value, wv),
-        (w_forget.at[pl.ds(row_at, rows), :], wf),
+        (w_forget.at[:, pl.ds(row_at, rows)], wf),
         (keys_cache, keys),
         (gates_cache, gates),
         (values_cache, values),
@@ -254,8 +257,13 @@
         )
     pl.semaphore_wait(barrier, n_kv + n_tp - 2)
 
+    turn = 2 * (kv // (n_kv // 2)) - 1
+
+    def kv_peer(j):
+        return lax.rem(kv + turn * j + n_kv, n_kv)
+
     def over_kv(phase, j, source, landing):
-        peer = lax.rem(kv + j, n_kv)
+        peer = kv_peer(j)
         return pltpu.make_async_remote_copy(
             src_ref=source(peer),
             dst_ref=landing.at[kv],
@@ -266,7 +274,7 @@
         )
 
     def from_kv(phase, j, source, landing):
-        peer = lax.rem(kv + n_kv - j, n_kv)
+        peer = lax.rem(kv - turn * j + n_kv, n_kv)
         pltpu.make_async_remote_copy(
             src_ref=source(peer),
             dst_ref=landing.at[peer],
@@ -312,20 +320,35 @@
         copy.start()
         pending.append(copy)
 
+    def share_squares(which, block):
+        column = jnp.sum(block * block, axis=-1, keepdims=True)
+        s_send[which] = to_row(column)
+        for j in range(1, n_kv):
+            send_kv(6 + which, j, lambda peer: s_send.at[which], s_all.at[which])
+        s_all[which, kv] = s_send[which]
+
+    def joined_squares(which):
+        for j in range(1, n_kv):
+            from_kv(6 + which, j, lambda peer: s_send.at[which], s_all.at[which])
+        total = s_all[which, 0]
+        for o in range(1, n_kv):
+            total = total + s_all[which, o]
+        return to_column(total, seqs)
+
     for j in range(1, n_tp):
         send_tp(0, j, lambda peer: tokens, tok_all)
     tok_all[tp] = tokens[...]
-    gain_a = gain_attn[:, pl.ds(row_at, rows)].astype(f32)
-    gain_m = gain_mixer[:, pl.ds(row_at, rows)].astype(f32)
+    gain_a = gain_attn[pl.ds(row_at, rows)].astype(f32).reshape(1, rows)
+    gain_m = gain_mixer[pl.ds(row_at, rows)].astype(f32).reshape(1, rows)
     for j in range(1, n_tp):
         from_tp(0, j, lambda peer: tokens, tok_all)
     tok = jnp.concatenate([tok_all[t] for t in range(n_tp)], axis=1).astype(f32)
     scaled = (tok * gain_a).astype(bf16)
 
+    share_squares(0, tok)
+
     ld_q.wait()
-    squares = split_squares(tok)
-    q_send[:, :cols] = jnp.dot(scaled, wq[...], preferred_element_type=f32).astype(bf16)
-    q_send[:, cols:] = squares.astype(bf16)
+    q_send[...] = jnp.dot(scaled, wq[...], preferred_element_type=f32).astype(bf16)
     for j in range(1, n_kv):
         send_kv(0, j, lambda peer: q_send, q_all)
     q_all[kv] = q_send[...]
@@ -335,7 +358,9 @@
     ld_f.wait()
     part_key = jnp.dot(scaled, wk[...], preferred_element_type=f32)
     part_value = jnp.dot(scaled, wv[...], preferred_element_type=f32)
-    part_gate = jnp.dot(scaled, wf[...], preferred_element_type=f32)
+    part_gate = lax.dot_general(
+        scaled, wf[...], (((1,), (1,)), ((), ())), preferred_element_type=f32
+    )
     for o in range(n_kv):
         at = slice(o * mine, (o + 1) * mine)
         p_send[o, :, :cols] = part_key[at]
@@ -351,8 +376,8 @@
     q_total = q_all[0].astype(f32)
     for o in range(1, n_kv):
         q_total = q_total + q_all[o].astype(f32)
-    attn_scale = lax.rsqrt(joined_squares(q_total[:, cols:]) / width + norm_eps)
-    query[:, :cols] = (attn_scale * q_total[:, :cols]).astype(bf16).astype(f32)
+    attn_scale = lax.rsqrt(joined_squares(0) / width + norm_eps)
+    query[:, :cols] = (attn_scale * q_total).astype(bf16).astype(f32)
     query[:, cols:] = jnp.broadcast_to(attn_scale, (seqs, LANES))
 
     ld_keys.wait()
@@ -395,7 +420,7 @@
             a_send[owner, r : r + 1, cols:] = jnp.sum(stats, axis=0, keepdims=True)
 
     def attend_for(j, carry):
-        attend(lax.rem(kv + j, n_kv))
+        attend(kv_peer(j))
         over_kv(2, j, lambda peer: a_send.at[peer], a_all).start()
         return carry
 
@@ -480,17 +505,16 @@
         res[t] = residual[:, t * piece : (t + 1) * piece]
 
     scaled_mid = (residual * gain_m).astype(bf16)
-    squares_mid = split_squares(residual).astype(bf16)
+    share_squares(1, residual)
 
     def up_piece(owner):
         at = pl.multiple_of(owner * unit, unit)
-        u_send[owner, :, :unit] = jnp.dot(
+        u_send[owner] = jnp.dot(
             scaled_mid, wu[:, pl.ds(at, unit)], preferred_element_type=f32
         ).astype(bf16)
-        u_send[owner, :, unit:] = squares_mid
-
-    for j in range(1, n_kv):
-        up_piece(lax.rem(kv + j, n_kv))
+
+    for j in range(1, n_kv):
+        up_piece(kv_peer(j))
         send_kv(4, j, lambda peer: u_send.at[peer], u_all)
     up_piece(kv)
     u_all[kv] = u_send[kv]
@@ -499,8 +523,8 @@
     up_total = u_all[0].astype(f32)
     for o in range(1, n_kv):
         up_total = up_total + u_all[o].astype(f32)
-    mixer_scale = lax.rsqrt(joined_squares(up_total[:, unit:]) / width + norm_eps)
-    active = jnp.maximum(mixer_scale * up_total[:, :unit], 0.0)
+    mixer_scale = lax.rsqrt(joined_squares(1) / width + norm_eps)
+    active = jnp.maximum(mixer_scale * up_total, 0.0)
     h_send[...] = (active * active).astype(bf16)
     for j in range(1, n_kv):
         send_kv(5, j, lambda peer: h_send, h_all)
@@ -564,7 +588,8 @@
         and 3 * heads <= LANES
         and all_heads < LANES
         and w_out.shape == (cols, rows)
-        and n_kv > 1
+        and seqs <= LANES
+        and n_kv % 2 == 0
         and n_tp > 1
     )
     if not fits:
@@ -586,7 +611,7 @@
             like(w_query),
             like(w_key),
             like(w_value),
-            pltpu.VMEM((rows, all_heads), bf16),
+            pltpu.VMEM((all_heads, rows), bf16),
             like(keys_cache),
             like(values_cache),
             like(gates_cache),
@@ -594,8 +619,8 @@
             like(w_up),
             like(w_down),
             pltpu.VMEM((n_tp, seqs, piece), bf16),
-            pltpu.VMEM((seqs, cols + LANES), bf16),
-            pltpu.VMEM((n_kv, seqs, cols + LANES), bf16),
+            pltpu.VMEM((seqs, cols), bf16),
+            pltpu.VMEM((n_kv, seqs, cols), bf16),
             pltpu.VMEM((n_kv, mine, 2 * cols + LANES), f32),
             pltpu.VMEM((n_kv, mine, 2 * cols + LANES), f32),
             pltpu.VMEM((n_kv, mine, cols + LANES), f32),
@@ -604,8 +629,8 @@
             pltpu.VMEM((n_kv, mine, cols), f32),
             pltpu.VMEM((seqs, rows), bf16),
             pltpu.VMEM((n_tp, seqs, rows), bf16),
-            pltpu.VMEM((n_kv, seqs, unit + LANES), bf16),
-            pltpu.VMEM((n_kv, seqs, unit + LANES), bf16),
+            pltpu.VMEM((n_kv, seqs, unit), bf16),
+            pltpu.VMEM((n_kv, seqs, unit), bf16),
             pltpu.VMEM((seqs, unit), bf16),
             pltpu.VMEM((n_kv, seqs, unit), bf16),
             pltpu.VMEM((n_tp, seqs, piece), f32),
@@ -613,9 +638,11 @@
             pltpu.VMEM((seqs, cols + LANES), f32),
             pltpu.VMEM((seqs, cols), f32),
             pltpu.VMEM((n_tp, seqs, piece), f32),
+            pltpu.VMEM((2, 1, LANES), f32),
+            pltpu.VMEM((2, n_kv, 1, LANES), f32),
             pltpu.SemaphoreType.DMA((10,)),
-            pltpu.SemaphoreType.DMA((6, n_kv)),
-            pltpu.SemaphoreType.DMA((6, n_kv)),
+            pltpu.SemaphoreType.DMA((8, n_kv)),
+            pltpu.SemaphoreType.DMA((8, n_kv)),
             pltpu.SemaphoreType.DMA((3, n_tp)),
             pltpu.SemaphoreType.DMA((3, n_tp)),
         ],
@@ -624,14 +651,14 @@
         ),
     )(
         tokens,
-        gain_attn.reshape(1, -1),
+        gain_attn,
         forget_bias.reshape(1, -1),
         lengths,
-        gain_mixer.reshape(1, -1),
+        gain_mixer,
         w_query,
         w_key,
         w_value,
-        w_forget,
+        w_forget.T,
         keys_cache,
         values_cache,
         gates_cache,

time: 54.8 us -> 48.3 us (0.88)
  local copies, waits for them, and re-layouts: 6.16 us -> 1.28 us
  Pallas kernels: 48.2 us -> 46.8 us
    reshape x2 -> x0, local copies, waits for them, and re-layouts: 2.61 us -> none  [the longest x1 1.3 us: layer(): gain_attn.reshape(1, -1)]
    unnamed x2 -> x1, local copies, waits for them, and re-layouts: 3.55 us -> 1.28 us
    pallas_call x1, Pallas kernels: 48.2 us -> 46.8 us  [layer(): pl.pallas_call(functools.partial(fused, n_kv, n_tp), out_shape=jax.ShapeD...]
where the time goes in v2:
time: 48.3 us; the launch traced here: 48.1 us
  Pallas kernels  46.8 us (97%)
  local copies, waits for them, and re-layouts  1.28 us (3%)
    pallas_call x1, Pallas kernels, layer(): pl.pallas_call(functools.partial(fused, n_kv, n_tp), out_shape=jax.ShapeD...  46.8 us
    unnamed x1, local copies, waits for them, and re-layouts  1.28 us

profile of v2, /device:TPU:0, one launch (start us, length us, event | category | flops | bytes accessed | tf_op | source)
XLA Modules:
  0.0 48.1 jit_solution(16426859902299900190)
XLA Ops:
  0.0 46.8 %shard_map.145 = bf16[16,128]{1,0:T(8,128)(2,1)} custom-call(bf16[16,128]{1,0:T(8,128)(2,1)} %tokens.1, bf16[4096]{0:T(1024)(128)(2,1)} %gain_attn.1, f32[1,32]{1,0:T(1,128)} %bitcast.3, s32[16]{0:T(128)} %lengths.1, bf16[4096]{0:T(1024)(128)(2,1)} %gain_mixer.1, bf16[512,512]{1,0:T(8,128)(2,1)} %w_query.1, bf16[512,512]{1,0:T(8,128)(2,1)} %w_key.1, ...), custom_call_target="tpu_custom_call" | custom-call | tf_op jit(solution)/shard_map/pallas_call | solution.py:605
  46.8 1.3 %copy.17 = bf16[16,128]{1,0:T(8,128)(2,1)} copy(bf16[16,128]{1,0:T(8,128)(2,1)} %shard_map.145) | data formatting | bytes 8192
